TPU v7x, 32 devices: a whole 2x2x4 slice. The times are simulated.
32 devices in a mesh: pp: 4 (over y, x), fs: 4 (over z), tp: 2 (over core).
Axes of the slice: x: 2, y: 2, z: 4, core: 2. Of those that a mesh axis runs over, the one named last changes fastest.
Arguments:
- micro_in: bfloat16 [2, 96, 1024], P(None, 'pp', ('tp', 'fs')), may hold values from -6 to 6
- norm_gain: float32 [4, 1024], P('pp'), may hold values from 0.5 to 1.5
- proj_gate: bfloat16 [4, 1024, 8, 4, 64], P('pp', None, 'tp', 'fs'), may hold values from -0.1875 to 0.1875
- proj_value: bfloat16 [4, 1024, 8, 4, 64], P('pp', None, 'tp', 'fs'), may hold values from -0.1875 to 0.1875
- proj_write: bfloat16 [4, 1024, 8, 128], P('pp', None, 'tp'), may hold values from -0.1875 to 0.1875
- proj_read: bfloat16 [4, 1024, 8, 128], P('pp', None, 'tp'), may hold values from -0.1875 to 0.1875
- proj_step: bfloat16 [4, 1024, 2, 8, 4], P('pp', None, None, 'tp', 'fs'), may hold values from -0.1875 to 0.1875
- step_bias: float32 [4, 2, 8, 4], P('pp', None, 'tp', 'fs'), may hold values from -4.6 to -2.3
- decay_log: float32 [4, 2, 8, 4], P('pp', None, 'tp', 'fs'), may hold values from 0 to 2.77
- skip_gain: float32 [4, 8, 4], P('pp', 'tp', 'fs'), may hold values from 0.5 to 1.5
- conv_value: float32 [4, 5, 8, 4, 64], P('pp', None, 'tp', 'fs'), may hold values from -2.5 to 2.5
- conv_write: float32 [4, 5, 8, 128], P('pp', None, 'tp'), may hold values from -2.5 to 2.5
- conv_read: float32 [4, 5, 8, 128], P('pp', None, 'tp'), may hold values from -2.5 to 2.5
- proj_out: bfloat16 [4, 8, 4, 64, 1024], P('pp', 'tp', 'fs'), may hold values from -0.125 to 0.125
Outputs:
- mixed_out: bfloat16 [2, 96, 1024], P(None, 'pp', ('tp', 'fs'))
All inputs are finite; a program needn't handle non-finite values.
Results may differ from a plain program's by a relative error of at most 0.025.
Values may be sent and summed in bfloat16 or wider, within the bound.
A program may use at most 64 MiB of HBM per device.

v0:
```python
import jax
import jax.numpy as jnp
from jax import lax
from jax.sharding import PartitionSpec as P

epsilon = 1e-06


def own_rows_2(portion, span, axis):
    count = span * lax.axis_size(axis)
    sent = portion(jnp.int32(0), count).astype(jnp.bfloat16)
    return lax.psum_scatter(sent, axis, scatter_dimension=0, tiled=True).astype(jnp.float32)


def from_behind(block, axis, distance):
    devices = range(lax.axis_size(axis))
    route = [(i - distance, i) for i in devices if i - distance in devices]
    return lax.ppermute(block, axis, route)


def spread(value, axis, source):
    kept = jnp.where(lax.axis_index(axis) == source, value, 0).astype(value.dtype)
    return lax.psum(kept, axis)


def centred_conv(signal, conv_taps):
    span_width = conv_taps.shape[0]
    half_width = span_width // 2
    length = signal.shape[0]
    padded = jnp.pad(signal, ((half_width, half_width), (0, 0)))
    running = jnp.zeros_like(signal)
    for offset in range(span_width):
        running = running + padded[offset : offset + length] * conv_taps[offset]
    return running


def duality_mix(
    gate_flat,
    value_flat,
    write_flat,
    read_flat,
    step_raw,
    step_bias,
    decay_log,
    skip_gain,
    conv_value,
    conv_write,
    conv_read,
):
    groups, per_group = skip_gain.shape
    length = gate_flat.shape[0]
    head_size = value_flat.shape[1] // (groups * per_group)
    state_size = write_flat.shape[1] // groups
    taps_count = conv_value.shape[0]
    value_act = jax.nn.silu(
        centred_conv(value_flat.astype(jnp.float32), conv_value.reshape(taps_count, -1))
    ).astype(jnp.bfloat16)
    write_act = jax.nn.silu(
        centred_conv(write_flat.astype(jnp.float32), conv_write.reshape(taps_count, -1))
    ).astype(jnp.bfloat16)
    read_act = jax.nn.silu(
        centred_conv(read_flat.astype(jnp.float32), conv_read.reshape(taps_count, -1))
    ).astype(jnp.bfloat16)
    step_size = jax.nn.softplus(step_raw.reshape(length, 2, groups, per_group) + step_bias[None])
    log_decay = step_size * (-jnp.exp(decay_log))[None]
    fwd_cum = jnp.cumsum(log_decay[:, 0], axis=0)
    bwd_cum = jnp.flip(jnp.cumsum(jnp.flip(log_decay[:, 1], 0), axis=0), 0)
    positions = jnp.arange(length)
    lower_mask = (positions[:, None] >= positions[None, :])[:, :, None, None]
    upper_mask = (positions[:, None] <= positions[None, :])[:, :, None, None]
    fwd_weight = (
        jnp.exp(jnp.where(lower_mask, fwd_cum[:, None] - fwd_cum[None, :], -jnp.inf))
        * step_size[None, :, 0]
    )
    bwd_weight = (
        jnp.exp(jnp.where(upper_mask, bwd_cum[:, None] - bwd_cum[None, :], -jnp.inf))
        * step_size[None, :, 1]
    )
    scores = jnp.einsum(
        "tgn,sgn->tsg",
        read_act.reshape(length, groups, state_size),
        write_act.reshape(length, groups, state_size),
        preferred_element_type=jnp.float32,
    )
    combined = scores[:, :, :, None] * (fwd_weight + bwd_weight)
    value_heads = value_act.reshape(length, groups, per_group, head_size).astype(jnp.float32)
    mixed_heads = jnp.einsum(
        "tsgh,sghp->tghp", combined, value_heads, precision=lax.Precision.HIGHEST
    )
    mixed_heads = mixed_heads + skip_gain[None, :, :, None] * value_heads
    return (mixed_heads.reshape(length, -1) * jax.nn.silu(gate_flat.astype(jnp.float32))).astype(
        jnp.bfloat16
    )


def body(
    micro_in,
    norm_gain,
    proj_gate,
    proj_value,
    proj_write,
    proj_read,
    proj_step,
    step_bias,
    decay_log,
    skip_gain,
    conv_value,
    conv_write,
    conv_read,
    proj_out,
):
    section_count = lax.axis_size("pp")
    section_idx = lax.axis_index("pp")
    width_model = norm_gain.shape[1]
    fed_blocks = lax.all_gather(micro_in, "pp", axis=1, tiled=True)
    micro_count = fed_blocks.shape[0]
    length = fed_blocks.shape[1]
    fed_columns = jnp.swapaxes(fed_blocks, 1, 2)
    gain_vec = norm_gain[0].astype(jnp.float32)
    cut_gate = proj_gate.shape[2] * proj_gate.shape[3] * proj_gate.shape[4]
    cut_write = proj_write.shape[2] * proj_write.shape[3]
    weight_all = jnp.concatenate(
        [
            proj_gate[0].reshape(width_model, -1),
            proj_value[0].reshape(width_model, -1),
            proj_write[0].reshape(width_model, -1),
            proj_read[0].reshape(width_model, -1),
            proj_step[0].reshape(width_model, -1),
        ],
        axis=1,
    )
    out_weights = proj_out[0].reshape(-1, width_model)
    own_rows = width_model // lax.axis_size(("tp", "fs"))

    def project(column_block):
        gathered = lax.all_gather(column_block, ("tp", "fs"), axis=0, tiled=True)
        as_float = gathered.astype(jnp.float32)
        scale_rms = lax.rsqrt(jnp.mean(as_float * as_float, axis=0) + epsilon)
        normed = (as_float * scale_rms[None, :] * gain_vec[:, None]).astype(jnp.bfloat16)
        return lax.dot_general(
            normed, weight_all, (((0,), (0,)), ((), ())), preferred_element_type=jnp.float32
        )

    def term_maker(token_rows):

        def term_rows(offset, span_count):
            weight_cols = lax.dynamic_slice_in_dim(out_weights, offset, span_count, 1)
            return lax.dot_general(
                weight_cols,
                token_rows,
                (((0,), (1,)), ((), ())),
                preferred_element_type=jnp.float32,
            )

        return term_rows

    def mix_block(column_block):
        projected = project(column_block)
        gate_flat = projected[:, :cut_gate].astype(jnp.bfloat16)
        value_flat = projected[:, cut_gate : 2 * cut_gate].astype(jnp.bfloat16)
        write_flat = projected[:, 2 * cut_gate : 2 * cut_gate + cut_write].astype(jnp.bfloat16)
        read_flat = projected[:, 2 * cut_gate + cut_write : 2 * cut_gate + 2 * cut_write].astype(
            jnp.bfloat16
        )
        step_raw = projected[:, 2 * cut_gate + 2 * cut_write :]
        gated_out = duality_mix(
            gate_flat,
            value_flat,
            write_flat,
            read_flat,
            step_raw,
            step_bias[0],
            decay_log[0],
            skip_gain[0],
            conv_value[0],
            conv_write[0],
            conv_read[0],
        )
        summed = own_rows_2(term_maker(gated_out), own_rows, ("tp", "fs"))
        branch = lax.optimization_barrier(summed.astype(jnp.bfloat16))
        return (column_block.astype(jnp.float32) + 0.5 * branch.astype(jnp.float32)).astype(
            jnp.bfloat16
        )

    total_steps = micro_count + section_count - 1

    def advance(moment, loop_state):
        arriving, collected = loop_state
        pick_index = jnp.clip(moment, 0, micro_count - 1)
        fresh_block = lax.dynamic_index_in_dim(fed_columns, pick_index, 0, keepdims=False)
        current = jnp.where(section_idx == 0, fresh_block, arriving)
        produced = mix_block(current)
        slot_index = moment - section_idx
        keep_flag = (
            (section_idx == section_count - 1) & (slot_index >= 0) & (slot_index < micro_count)
        )
        slot_safe = jnp.clip(slot_index, 0, micro_count - 1)
        previous = lax.dynamic_index_in_dim(collected, slot_safe, 0, keepdims=False)
        collected = lax.dynamic_update_index_in_dim(
            collected, jnp.where(keep_flag, produced, previous), slot_safe, 0
        )
        arriving = from_behind(produced, "pp", 1)
        return (arriving, collected)

    start_loop = (jnp.zeros_like(fed_columns[0]), jnp.zeros_like(fed_columns))
    arriving, collected = lax.fori_loop(0, total_steps, advance, start_loop)
    shared = spread(collected, "pp", section_count - 1)
    token_share = length // section_count
    own_block = lax.dynamic_slice_in_dim(shared, section_idx * token_share, token_share, 2)
    as_float = own_block.astype(jnp.float32)
    partial_squares = jnp.sum(as_float * as_float, axis=1)
    total_squares = lax.psum(partial_squares, ("tp", "fs"))
    scale_rms = lax.rsqrt(total_squares / width_model + epsilon)
    result = (as_float * scale_rms[:, None, :]).astype(jnp.bfloat16)
    return jnp.swapaxes(result, 1, 2)


def solution(mesh):
    return jax.shard_map(
        body,
        mesh=mesh,
        in_specs=(
            P(None, "pp", ("tp", "fs")),
            P("pp", None),
            P("pp", None, "tp", "fs", None),
            P("pp", None, "tp", "fs", None),
            P("pp", None, "tp", None),
            P("pp", None, "tp", None),
            P("pp", None, None, "tp", "fs"),
            P("pp", None, "tp", "fs"),
            P("pp", None, "tp", "fs"),
            P("pp", "tp", "fs"),
            P("pp", None, "tp", "fs", None),
            P("pp", None, "tp", None),
            P("pp", None, "tp", None),
            P("pp", "tp", "fs", None, None),
        ),
        out_specs=P(None, "pp", ("tp", "fs")),
        check_vma=False,
    )
```

profile of v0, /device:TPU:1, one launch (start us, length us, event | category | flops | bytes accessed | tf_op | source)
XLA Modules:
  0.0 505.2 jit_solution(10900077778748892538)
XLA Ops:
  16.3 8.0 %all_gather.13 = bf16[2,96,128]{2,1,0:T(8,128)(2,1)} all-gather(bf16[2,24,128]{2,1,0:T(8,128)(2,1)S(1)} %copy-done.6), channel_id=1, replica_groups=mesh['pp'=4,'fs'=4,'tp'=2] {'pp'}, dimensions={1}, use_global_device_ids=true | all-gather | bytes 61440 | tf_op jit(solution)/shard_map/all_gather | solution.py:115
  25.6 438.8 %while.17 = (s32[]{:T(128)}, bf16[128,96]{0,1:T(8,128)(2,1)S(1)}, bf16[2,128,96]{1,2,0:T(8,128)(2,1)}, pred[]{:T(512)}, bf16[2,128,96]{1,2,0:T(8,128)(2,1)}, /*i...) while((s32[]{:T(128)}, bf16[128,96]{0,1:T(8,128)(2,1)S(1)}, ...), condition=%wide.region_5.6_spmd, body=%wide.region_0.5_spmd.sunk | while | flops 395120736 | bytes 11393579 | solution.py:206
  27.0 24.4 %all_gather.15 = bf16[1024,96]{0,1:T(8,128)(2,1)S(1)} all-gather(bf16[128,96]{0,1:T(8,128)(2,1)S(1)} %bitcast_select_fusion.3), channel_id=1, replica_groups=mesh['pp'=4,'fs'=4,'tp'=2] {'tp','fs'}, dimensions={0}, use_global_device_ids=true | all-gather | bytes 221184 | tf_op jit(solution)/shard_map/while/body/eval_jaxpr/all_gather | solution.py:136
  51.5 2.3 fusion.90
  77.5 29.5 %reduce-scatter.6.cloned.1.call-done = bf16[128,96]{1,0:T(8,128)(2,1)} async-done(((bf16[1024,96]{1,0:T(8,128)(2,1)}), bf16[128,96]{1,0:T(8,128)(2,1)}) %reduce-scatter.6.cloned.1.call-update) | async-done | bytes 24592 | tf_op jit(solution)/shard_map/while
  109.2 3.1 collective-permute-start
  114.6 22.9 %all_gather.15 = bf16[1024,96]{0,1:T(8,128)(2,1)S(1)} all-gather(bf16[128,96]{0,1:T(8,128)(2,1)S(1)} %bitcast_select_fusion.3), channel_id=1, replica_groups=mesh['pp'=4,'fs'=4,'tp'=2] {'tp','fs'}, dimensions={0}, use_global_device_ids=true | all-gather | bytes 221184 | tf_op jit(solution)/shard_map/while/body/eval_jaxpr/all_gather | solution.py:136
  137.6 2.3 fusion.90
  163.7 31.1 %reduce-scatter.6.cloned.1.call-done = bf16[128,96]{1,0:T(8,128)(2,1)} async-done(((bf16[1024,96]{1,0:T(8,128)(2,1)}), bf16[128,96]{1,0:T(8,128)(2,1)}) %reduce-scatter.6.cloned.1.call-update) | async-done | bytes 24592 | tf_op jit(solution)/shard_map/while
  197.0 3.1 collective-permute-start
  202.4 22.6 %all_gather.15 = bf16[1024,96]{0,1:T(8,128)(2,1)S(1)} all-gather(bf16[128,96]{0,1:T(8,128)(2,1)S(1)} %bitcast_select_fusion.3), channel_id=1, replica_groups=mesh['pp'=4,'fs'=4,'tp'=2] {'tp','fs'}, dimensions={0}, use_global_device_ids=true | all-gather | bytes 221184 | tf_op jit(solution)/shard_map/while/body/eval_jaxpr/all_gather | solution.py:136
  225.2 2.3 fusion.90
  251.3 31.2 %reduce-scatter.6.cloned.1.call-done = bf16[128,96]{1,0:T(8,128)(2,1)} async-done(((bf16[1024,96]{1,0:T(8,128)(2,1)}), bf16[128,96]{1,0:T(8,128)(2,1)}) %reduce-scatter.6.cloned.1.call-update) | async-done | bytes 24592 | tf_op jit(solution)/shard_map/while
  284.7 3.1 collective-permute-start
  290.1 22.8 %all_gather.15 = bf16[1024,96]{0,1:T(8,128)(2,1)S(1)} all-gather(bf16[128,96]{0,1:T(8,128)(2,1)S(1)} %bitcast_select_fusion.3), channel_id=1, replica_groups=mesh['pp'=4,'fs'=4,'tp'=2] {'tp','fs'}, dimensions={0}, use_global_device_ids=true | all-gather | bytes 221184 | tf_op jit(solution)/shard_map/while/body/eval_jaxpr/all_gather | solution.py:136
  313.0 2.3 fusion.90
  339.1 31.2 %reduce-scatter.6.cloned.1.call-done = bf16[128,96]{1,0:T(8,128)(2,1)} async-done(((bf16[1024,96]{1,0:T(8,128)(2,1)}), bf16[128,96]{1,0:T(8,128)(2,1)}) %reduce-scatter.6.cloned.1.call-update) | async-done | bytes 24592 | tf_op jit(solution)/shard_map/while
  372.5 3.1 collective-permute-start
  377.9 22.8 %all_gather.15 = bf16[1024,96]{0,1:T(8,128)(2,1)S(1)} all-gather(bf16[128,96]{0,1:T(8,128)(2,1)S(1)} %bitcast_select_fusion.3), channel_id=1, replica_groups=mesh['pp'=4,'fs'=4,'tp'=2] {'tp','fs'}, dimensions={0}, use_global_device_ids=true | all-gather | bytes 221184 | tf_op jit(solution)/shard_map/while/body/eval_jaxpr/all_gather | solution.py:136
  400.8 2.3 fusion.90
  426.9 31.3 %reduce-scatter.6.cloned.1.call-done = bf16[128,96]{1,0:T(8,128)(2,1)} async-done(((bf16[1024,96]{1,0:T(8,128)(2,1)}), bf16[128,96]{1,0:T(8,128)(2,1)}) %reduce-scatter.6.cloned.1.call-update) | async-done | bytes 24592 | tf_op jit(solution)/shard_map/while
  460.3 3.1 collective-permute-start
  464.3 14.2 %psum.14 = bf16[2,128,96]{1,2,0:T(8,128)(2,1)S(1)} all-reduce(bf16[2,128,96]{1,2,0:T(8,128)(2,1)S(1)} %broadcast_select_fusion), channel_id=1, replica_groups=mesh['pp'=4,'fs'=4,'tp'=2] {'pp'}, use_global_device_ids=true, to_apply=%region_6.7 | all-reduce | flops 24576 | bytes 98304 | tf_op jit(solution)/shard_map/psum | solution.py:23
  478.7 19.4 %psum.15 = f32[2,24]{1,0:T(2,128)S(1)} all-reduce(f32[2,24]{1,0:T(2,128)S(1)} %fusion.49), channel_id=1, replica_groups=mesh['pp'=4,'fs'=4,'tp'=2] {'tp','fs'}, use_global_device_ids=true, to_apply=%region_8.9 | all-reduce | flops 48 | bytes 384 | tf_op jit(solution)/shard_map/psum | solution.py:212
  (259 shorter events, 153.5 us)
Async XLA Ops:
  9.6 4.8 copy-start.5
  9.7 6.7 %copy-start.6 = (bf16[2,24,128]{2,1,0:T(8,128)(2,1)S(1)}, bf16[2,24,128]{2,1,0:T(8,128)(2,1)}, u32[]{:S(2)}) copy-start(bf16[2,24,128]{2,1,0:T(8,128)(2,1)} %param.16) | copy-start | bytes 36868
  9.7 14.7 %copy-start.7 = (f32[1,2,4,1]{2,3,1,0:T(1,128)S(1)}, f32[1,2,4,1]{2,3,1,0:T(1,128)}, u32[]{:S(2)}) copy-start(f32[1,2,4,1]{2,3,1,0:T(1,128)} %param.24) | copy-start | bytes 100
  25.6 81.4 %reduce-scatter.6.cloned.1.call-start = ((), (), s32[]{:S(2)}) async-start(), calls=%async_computation.1 | async-start | bytes 294912 | tf_op jit(solution)/shard_map/while
  27.0 24.5 %copy-start.3 = (bf16[128,96]{0,1:T(8,128)(2,1)}, bf16[128,96]{0,1:T(8,128)(2,1)S(1)}, u32[]{:S(2)}) copy-start(bf16[128,96]{0,1:T(8,128)(2,1)S(1)} %bitcast_select_fusion.3) | copy-start | bytes 73732 | tf_op jit(solution)/shard_map/while
  68.2 3.1 copy-start.1
  68.2 3.1 copy-start.2
  109.2 4.0 collective-permute-start
  113.2 81.6 %reduce-scatter.6.cloned.1.call-start = ((), (), s32[]{:S(2)}) async-start(), calls=%async_computation.1 | async-start | bytes 294912 | tf_op jit(solution)/shard_map/while
  114.6 23.0 %copy-start.3 = (bf16[128,96]{0,1:T(8,128)(2,1)}, bf16[128,96]{0,1:T(8,128)(2,1)S(1)}, u32[]{:S(2)}) copy-start(bf16[128,96]{0,1:T(8,128)(2,1)S(1)} %bitcast_select_fusion.3) | copy-start | bytes 73732 | tf_op jit(solution)/shard_map/while
  154.4 3.1 copy-start.2
  197.0 4.0 collective-permute-start
  201.0 81.4 %reduce-scatter.6.cloned.1.call-start = ((), (), s32[]{:S(2)}) async-start(), calls=%async_computation.1 | async-start | bytes 294912 | tf_op jit(solution)/shard_map/while
  202.4 22.8 %copy-start.3 = (bf16[128,96]{0,1:T(8,128)(2,1)}, bf16[128,96]{0,1:T(8,128)(2,1)S(1)}, u32[]{:S(2)}) copy-start(bf16[128,96]{0,1:T(8,128)(2,1)S(1)} %bitcast_select_fusion.3) | copy-start | bytes 73732 | tf_op jit(solution)/shard_map/while
  242.0 3.1 copy-start.2
  284.7 4.0 collective-permute-start
  288.7 81.6 %reduce-scatter.6.cloned.1.call-start = ((), (), s32[]{:S(2)}) async-start(), calls=%async_computation.1 | async-start | bytes 294912 | tf_op jit(solution)/shard_map/while
  290.1 22.9 %copy-start.3 = (bf16[128,96]{0,1:T(8,128)(2,1)}, bf16[128,96]{0,1:T(8,128)(2,1)S(1)}, u32[]{:S(2)}) copy-start(bf16[128,96]{0,1:T(8,128)(2,1)S(1)} %bitcast_select_fusion.3) | copy-start | bytes 73732 | tf_op jit(solution)/shard_map/while
  329.8 3.1 copy-start.2
  372.5 4.0 collective-permute-start
  376.5 81.6 %reduce-scatter.6.cloned.1.call-start = ((), (), s32[]{:S(2)}) async-start(), calls=%async_computation.1 | async-start | bytes 294912 | tf_op jit(solution)/shard_map/while
  377.9 22.9 %copy-start.3 = (bf16[128,96]{0,1:T(8,128)(2,1)}, bf16[128,96]{0,1:T(8,128)(2,1)S(1)}, u32[]{:S(2)}) copy-start(bf16[128,96]{0,1:T(8,128)(2,1)S(1)} %bitcast_select_fusion.3) | copy-start | bytes 73732 | tf_op jit(solution)/shard_map/while
  417.6 3.1 copy-start.2
  460.3 4.0 collective-permute-start
  (10 other events, 19.4 us)
Sparse Core Ops, SparseCore 0:
  76.9 30.0 reduce-scatter.5
  163.0 31.6 reduce-scatter.5
  250.6 31.7 reduce-scatter.5
  338.4 31.7 reduce-scatter.5
  426.2 31.8 reduce-scatter.5
where the time goes:
time: 509 us; the launch traced here: 505 us
  waiting for transfers between devices  159 us (31%)
  blocking collectives  157 us (31%)
  local copies, waits for them, and re-layouts  86.1 us (17%)
  other arithmetic  37.1 us (7%)
  matrix products  37 us (7%)
  starting transfers between devices  15.4 us (3%)
  between operations  13.2 us (3%)
    while x10, waiting for transfers between devices  154 us
    all_gather x5, blocking collectives, project(): gathered = lax.all_gather(column_block, ('tp', 'fs'), axis=0, tiled=True)  115 us
    mul x30, local copies, waits for them, and re-layouts, centred_conv(): running = running + padded[offset:offset + length] * conv_taps[offset]  20.8 us
    psum x1, blocking collectives, body(): total_squares = lax.psum(partial_squares, ('tp', 'fs'))  19.4 us
    rev x20, local copies, waits for them, and re-layouts, duality_mix(): bwd_cum = jnp.flip(jnp.cumsum(jnp.flip(log_decay[:, 1], 0), axis=0), 0)  17.8 us
    ppermute x5, starting transfers between devices, from_behind(): return lax.ppermute(block, axis, route)  15.4 us
    psum x1, blocking collectives, spread(): return lax.psum(kept, axis)  14.2 us
    while x50, local copies, waits for them, and re-layouts  13.1 us
  transfers between devices with their start and end apart: 10, of which 10 were waited for; matrix products, arithmetic and copies ran while one was open for 1% of the time, Pallas kernels for 0%

commit v1 on v0

--- a/solution.py
+++ b/solution.py
@@ -133,7 +133,12 @@
     own_rows = width_model // lax.axis_size(("tp", "fs"))
 
     def project(column_block):
-        gathered = lax.all_gather(column_block, ("tp", "fs"), axis=0, tiled=True)
+        gathered = jnp.concatenate(
+            lax.all_to_all(
+                jnp.stack([column_block] * lax.axis_size(("tp", "fs"))), ("tp", "fs"), 0, 0
+            ),
+            axis=0,
+        )
         as_float = gathered.astype(jnp.float32)
         scale_rms = lax.rsqrt(jnp.mean(as_float * as_float, axis=0) + epsilon)
         normed = (as_float * scale_rms[None, :] * gain_vec[:, None]).astype(jnp.bfloat16)

time: 509 us -> 441 us (0.87)
  blocking collectives: 157 us -> 41.5 us
  starting transfers between devices: 15.4 us -> 42.2 us
  waiting for transfers between devices: 159 us -> 182 us
    all_gather x5 -> x0, blocking collectives: 115 us -> none  [project(): gathered = lax.all_gather(column_block, ('tp', 'fs'), axis=0, tiled=True)]
    all_to_all x0 -> x5, starting transfers between devices: none -> 26.8 us  [project(): lax.all_to_all(jnp.stack([column_block] * lax.axis_size(('tp', 'fs'))), (...]
    all_to_all x0 -> x5, waiting for transfers between devices: none -> 25.6 us  [project(): lax.all_to_all(jnp.stack([column_block] * lax.axis_size(('tp', 'fs'))), (...]
    mul x30, local copies, waits for them, and re-layouts: 20.8 us -> 9.02 us  [centred_conv(): running = running + padded[offset:offset + length] * conv_taps[offset]]
  transfers between devices with their start and end apart: 10 -> 15, of which waited for: 10 -> 15; matrix products, arithmetic and copies ran while one was open for 1% -> 4% of each run, Pallas kernels for 0% -> 0%
where the time goes in v1:
time: 441 us; the launch traced here: 437 us
  waiting for transfers between devices  182 us (41%)
  local copies, waits for them, and re-layouts  83.8 us (19%)
  starting transfers between devices  42.2 us (10%)
  blocking collectives  41.5 us (9%)
  matrix products  38.3 us (9%)
  other arithmetic  35.4 us (8%)
  between operations  13.2 us (3%)
    while x10, waiting for transfers between devices  152 us
    all_to_all x5, starting transfers between devices, project(): lax.all_to_all(jnp.stack([column_block] * lax.axis_size(('tp', 'fs'))), (...  26.8 us
    all_to_all x5, waiting for transfers between devices, project(): lax.all_to_all(jnp.stack([column_block] * lax.axis_size(('tp', 'fs'))), (...  25.6 us
    psum x1, blocking collectives, body(): total_squares = lax.psum(partial_squares, ('tp', 'fs'))  19.3 us
    rev x20, local copies, waits for them, and re-layouts, duality_mix(): bwd_cum = jnp.flip(jnp.cumsum(jnp.flip(log_decay[:, 1], 0), axis=0), 0)  17.8 us
    while x50, local copies, waits for them, and re-layouts  16.1 us
    ppermute x5, starting transfers between devices, from_behind(): return lax.ppermute(block, axis, route)  15.3 us
    psum x1, blocking collectives, spread(): return lax.psum(kept, axis)  14.2 us
  transfers between devices with their start and end apart: 15, of which 15 were waited for; matrix products, arithmetic and copies ran while one was open for 4% of the time, Pallas kernels for 0%

profile of v1, /device:TPU:1, one launch (start us, length us, event | category | flops | bytes accessed | tf_op | source)
XLA Modules:
  0.0 436.7 jit_solution(9364202150992036408)
XLA Ops:
  16.4 8.0 %all_gather.3 = bf16[2,96,128]{2,1,0:T(8,128)(2,1)} all-gather(bf16[2,24,128]{2,1,0:T(8,128)(2,1)S(1)} %copy-done.8), channel_id=1, replica_groups=mesh['pp'=4,'fs'=4,'tp'=2] {'pp'}, dimensions={1}, use_global_device_ids=true | all-gather | bytes 61440 | tf_op jit(solution)/shard_map/all_gather | solution.py:115
  25.6 370.2 %while.17 = (s32[]{:T(128)}, bf16[128,96]{0,1:T(8,128)(2,1)S(1)}, bf16[2,128,96]{1,2,0:T(8,128)(2,1)}, pred[]{:T(512)}, bf16[2,128,96]{1,2,0:T(8,128)(2,1)}, /*i...) while((s32[]{:T(128)}, bf16[128,96]{0,1:T(8,128)(2,1)S(1)}, ...), condition=%wide.region_5.6_spmd, body=%wide.region_0.5_spmd.sunk | while | flops 395120736 | bytes 11988555 | solution.py:211
  27.7 7.2 %all-to-all-start = ((bf16[8,128,96]{1,2,0:T(8,128)(2,1)}), bf16[8,128,96]{1,2,0:T(8,128)(2,1)}, u32[]{:S(2)}, u32[]{:S(2)}) async-start(bf16[8,128,96]{1,2,0:T(8,128)(2,1)} %stack.7), calls=%async_computation | async-start | bytes 393216 | tf_op jit(solution)/shard_map/while/body/eval_jaxpr/all_to_all | solution.py:137
  37.5 5.1 %all-to-all-done = bf16[8,128,96]{1,2,0:T(8,128)(2,1)} async-done(((bf16[8,128,96]{1,2,0:T(8,128)(2,1)}), bf16[8,128,96]{1,2,0:T(8,128)(2,1)}, u32[]{:S(2)}, u32[]{:S(2)}) %all-to-all-start) | async-done | bytes 196640 | tf_op jit(solution)/shard_map/while/body/eval_jaxpr/all_to_all | solution.py:137
  65.0 28.9 %reduce-scatter.6.cloned.1.call-done = bf16[128,96]{1,0:T(8,128)(2,1)} async-done(((bf16[1024,96]{1,0:T(8,128)(2,1)}), bf16[128,96]{1,0:T(8,128)(2,1)}) %reduce-scatter.6.cloned.1.call-update) | async-done | bytes 24592 | tf_op jit(solution)/shard_map/while
  96.2 3.1 collective-permute-start
  102.2 4.9 %all-to-all-start = ((bf16[8,128,96]{1,2,0:T(8,128)(2,1)}), bf16[8,128,96]{1,2,0:T(8,128)(2,1)}, u32[]{:S(2)}, u32[]{:S(2)}) async-start(bf16[8,128,96]{1,2,0:T(8,128)(2,1)} %stack.7), calls=%async_computation | async-start | bytes 393216 | tf_op jit(solution)/shard_map/while/body/eval_jaxpr/all_to_all | solution.py:137
  109.8 5.1 %all-to-all-done = bf16[8,128,96]{1,2,0:T(8,128)(2,1)} async-done(((bf16[8,128,96]{1,2,0:T(8,128)(2,1)}), bf16[8,128,96]{1,2,0:T(8,128)(2,1)}, u32[]{:S(2)}, u32[]{:S(2)}) %all-to-all-start) | async-done | bytes 196640 | tf_op jit(solution)/shard_map/while/body/eval_jaxpr/all_to_all | solution.py:137
  137.3 30.6 %reduce-scatter.6.cloned.1.call-done = bf16[128,96]{1,0:T(8,128)(2,1)} async-done(((bf16[1024,96]{1,0:T(8,128)(2,1)}), bf16[128,96]{1,0:T(8,128)(2,1)}) %reduce-scatter.6.cloned.1.call-update) | async-done | bytes 24592 | tf_op jit(solution)/shard_map/while
  170.1 3.1 collective-permute-start
  176.1 4.9 %all-to-all-start = ((bf16[8,128,96]{1,2,0:T(8,128)(2,1)}), bf16[8,128,96]{1,2,0:T(8,128)(2,1)}, u32[]{:S(2)}, u32[]{:S(2)}) async-start(bf16[8,128,96]{1,2,0:T(8,128)(2,1)} %stack.7), calls=%async_computation | async-start | bytes 393216 | tf_op jit(solution)/shard_map/while/body/eval_jaxpr/all_to_all | solution.py:137
  183.6 5.1 %all-to-all-done = bf16[8,128,96]{1,2,0:T(8,128)(2,1)} async-done(((bf16[8,128,96]{1,2,0:T(8,128)(2,1)}), bf16[8,128,96]{1,2,0:T(8,128)(2,1)}, u32[]{:S(2)}, u32[]{:S(2)}) %all-to-all-start) | async-done | bytes 196640 | tf_op jit(solution)/shard_map/while/body/eval_jaxpr/all_to_all | solution.py:137
  211.1 30.6 %reduce-scatter.6.cloned.1.call-done = bf16[128,96]{1,0:T(8,128)(2,1)} async-done(((bf16[1024,96]{1,0:T(8,128)(2,1)}), bf16[128,96]{1,0:T(8,128)(2,1)}) %reduce-scatter.6.cloned.1.call-update) | async-done | bytes 24592 | tf_op jit(solution)/shard_map/while
  244.0 3.1 collective-permute-start
  250.0 4.9 %all-to-all-start = ((bf16[8,128,96]{1,2,0:T(8,128)(2,1)}), bf16[8,128,96]{1,2,0:T(8,128)(2,1)}, u32[]{:S(2)}, u32[]{:S(2)}) async-start(bf16[8,128,96]{1,2,0:T(8,128)(2,1)} %stack.7), calls=%async_computation | async-start | bytes 393216 | tf_op jit(solution)/shard_map/while/body/eval_jaxpr/all_to_all | solution.py:137
  257.6 5.1 %all-to-all-done = bf16[8,128,96]{1,2,0:T(8,128)(2,1)} async-done(((bf16[8,128,96]{1,2,0:T(8,128)(2,1)}), bf16[8,128,96]{1,2,0:T(8,128)(2,1)}, u32[]{:S(2)}, u32[]{:S(2)}) %all-to-all-start) | async-done | bytes 196640 | tf_op jit(solution)/shard_map/while/body/eval_jaxpr/all_to_all | solution.py:137
  285.1 30.6 %reduce-scatter.6.cloned.1.call-done = bf16[128,96]{1,0:T(8,128)(2,1)} async-done(((bf16[1024,96]{1,0:T(8,128)(2,1)}), bf16[128,96]{1,0:T(8,128)(2,1)}) %reduce-scatter.6.cloned.1.call-update) | async-done | bytes 24592 | tf_op jit(solution)/shard_map/while
  317.9 3.1 collective-permute-start
  324.0 4.9 %all-to-all-start = ((bf16[8,128,96]{1,2,0:T(8,128)(2,1)}), bf16[8,128,96]{1,2,0:T(8,128)(2,1)}, u32[]{:S(2)}, u32[]{:S(2)}) async-start(bf16[8,128,96]{1,2,0:T(8,128)(2,1)} %stack.7), calls=%async_computation | async-start | bytes 393216 | tf_op jit(solution)/shard_map/while/body/eval_jaxpr/all_to_all | solution.py:137
  331.5 5.1 %all-to-all-done = bf16[8,128,96]{1,2,0:T(8,128)(2,1)} async-done(((bf16[8,128,96]{1,2,0:T(8,128)(2,1)}), bf16[8,128,96]{1,2,0:T(8,128)(2,1)}, u32[]{:S(2)}, u32[]{:S(2)}) %all-to-all-start) | async-done | bytes 196640 | tf_op jit(solution)/shard_map/while/body/eval_jaxpr/all_to_all | solution.py:137
  359.0 30.6 %reduce-scatter.6.cloned.1.call-done = bf16[128,96]{1,0:T(8,128)(2,1)} async-done(((bf16[1024,96]{1,0:T(8,128)(2,1)}), bf16[128,96]{1,0:T(8,128)(2,1)}) %reduce-scatter.6.cloned.1.call-update) | async-done | bytes 24592 | tf_op jit(solution)/shard_map/while
  391.8 3.1 collective-permute-start
  395.8 14.2 %psum.14 = bf16[2,128,96]{1,2,0:T(8,128)(2,1)S(1)} all-reduce(bf16[2,128,96]{1,2,0:T(8,128)(2,1)S(1)} %broadcast_select_fusion), channel_id=1, replica_groups=mesh['pp'=4,'fs'=4,'tp'=2] {'pp'}, use_global_device_ids=true, to_apply=%region_6.7 | all-reduce | flops 24576 | bytes 98304 | tf_op jit(solution)/shard_map/psum | solution.py:23
  410.2 19.3 %psum.15 = f32[2,24]{1,0:T(2,128)S(1)} all-reduce(f32[2,24]{1,0:T(2,128)S(1)} %fusion.49), channel_id=1, replica_groups=mesh['pp'=4,'fs'=4,'tp'=2] {'tp','fs'}, use_global_device_ids=true, to_apply=%region_8.9 | all-reduce | flops 48 | bytes 384 | tf_op jit(solution)/shard_map/psum | solution.py:217
  (273 shorter events, 162.1 us)
Async XLA Ops:
  9.6 4.8 %copy-start.7 = (bf16[1,1024,2,4,1]{1,3,4,2,0:T(4,128)(2,1)S(1)}, bf16[1,1024,2,4,1]{1,3,4,2,0:T(4,128)(2,1)}, u32[]{:S(2)}) copy-start(bf16[1,1024,2,4,1]{1,3,4,2,0:T(4,128)(2,1)} %param.22) | copy-start | bytes 49156
  9.7 6.7 %copy-start.8 = (bf16[2,24,128]{2,1,0:T(8,128)(2,1)S(1)}, bf16[2,24,128]{2,1,0:T(8,128)(2,1)}, u32[]{:S(2)}) copy-start(bf16[2,24,128]{2,1,0:T(8,128)(2,1)} %param.16) | copy-start | bytes 36868
  9.7 14.7 %copy-start.9 = (f32[1,2,4,1]{2,3,1,0:T(1,128)S(1)}, f32[1,2,4,1]{2,3,1,0:T(1,128)}, u32[]{:S(2)}) copy-start(f32[1,2,4,1]{2,3,1,0:T(1,128)} %param.24) | copy-start | bytes 100
  9.7 15.9 %copy-start.5 = (f32[1,5,4,128]{3,2,1,0:T(4,128)S(1)}, f32[1,5,4,128]{3,2,1,0:T(4,128)}, u32[]{:S(2)}) copy-start(f32[1,5,4,128]{3,2,1,0:T(4,128)} %param.27) | copy-start | bytes 30724
  9.7 15.9 %copy-start.6 = (f32[1,1024]{1,0:T(1,128)S(1)}, f32[1,1024]{1,0:T(1,128)}, u32[]{:S(2)}) copy-start(f32[1,1024]{1,0:T(1,128)} %param.17) | copy-start | bytes 12292
  11.8 2.6 copy-start.4
  27.7 15.0 %all-to-all-start = ((bf16[8,128,96]{1,2,0:T(8,128)(2,1)}), bf16[8,128,96]{1,2,0:T(8,128)(2,1)}, u32[]{:S(2)}, u32[]{:S(2)}) async-start(bf16[8,128,96]{1,2,0:T(8,128)(2,1)} %stack.7), calls=%async_computation | async-start | bytes 393216 | tf_op jit(solution)/shard_map/while/body/eval_jaxpr/all_to_all | solution.py:137
  34.9 59.0 %reduce-scatter.6.cloned.1.call-start = ((), (), s32[]{:S(2)}) async-start(), calls=%async_computation.2 | async-start | bytes 294912 | tf_op jit(solution)/shard_map/while
  56.6 2.3 copy-start.2
  96.2 4.0 collective-permute-start
  102.2 12.6 %all-to-all-start = ((bf16[8,128,96]{1,2,0:T(8,128)(2,1)}), bf16[8,128,96]{1,2,0:T(8,128)(2,1)}, u32[]{:S(2)}, u32[]{:S(2)}) async-start(bf16[8,128,96]{1,2,0:T(8,128)(2,1)} %stack.7), calls=%async_computation | async-start | bytes 393216 | tf_op jit(solution)/shard_map/while/body/eval_jaxpr/all_to_all | solution.py:137
  107.1 60.7 %reduce-scatter.6.cloned.1.call-start = ((), (), s32[]{:S(2)}) async-start(), calls=%async_computation.2 | async-start | bytes 294912 | tf_op jit(solution)/shard_map/while
  128.8 2.3 copy-start.2
  170.1 4.0 collective-permute-start
  176.1 12.6 %all-to-all-start = ((bf16[8,128,96]{1,2,0:T(8,128)(2,1)}), bf16[8,128,96]{1,2,0:T(8,128)(2,1)}, u32[]{:S(2)}, u32[]{:S(2)}) async-start(bf16[8,128,96]{1,2,0:T(8,128)(2,1)} %stack.7), calls=%async_computation | async-start | bytes 393216 | tf_op jit(solution)/shard_map/while/body/eval_jaxpr/all_to_all | solution.py:137
  181.0 60.8 %reduce-scatter.6.cloned.1.call-start = ((), (), s32[]{:S(2)}) async-start(), calls=%async_computation.2 | async-start | bytes 294912 | tf_op jit(solution)/shard_map/while
  202.7 2.3 copy-start.2
  244.0 4.0 collective-permute-start
  250.0 12.6 %all-to-all-start = ((bf16[8,128,96]{1,2,0:T(8,128)(2,1)}), bf16[8,128,96]{1,2,0:T(8,128)(2,1)}, u32[]{:S(2)}, u32[]{:S(2)}) async-start(bf16[8,128,96]{1,2,0:T(8,128)(2,1)} %stack.7), calls=%async_computation | async-start | bytes 393216 | tf_op jit(solution)/shard_map/while/body/eval_jaxpr/all_to_all | solution.py:137
  254.9 60.8 %reduce-scatter.6.cloned.1.call-start = ((), (), s32[]{:S(2)}) async-start(), calls=%async_computation.2 | async-start | bytes 294912 | tf_op jit(solution)/shard_map/while
  317.9 4.0 collective-permute-start
  324.0 12.6 %all-to-all-start = ((bf16[8,128,96]{1,2,0:T(8,128)(2,1)}), bf16[8,128,96]{1,2,0:T(8,128)(2,1)}, u32[]{:S(2)}, u32[]{:S(2)}) async-start(bf16[8,128,96]{1,2,0:T(8,128)(2,1)} %stack.7), calls=%async_computation | async-start | bytes 393216 | tf_op jit(solution)/shard_map/while/body/eval_jaxpr/all_to_all | solution.py:137
  328.9 60.8 %reduce-scatter.6.cloned.1.call-start = ((), (), s32[]{:S(2)}) async-start(), calls=%async_computation.2 | async-start | bytes 294912 | tf_op jit(solution)/shard_map/while
  391.8 4.0 collective-permute-start
  (17 other events, 23.4 us)
Sparse Core Ops, SparseCore 0:
  64.4 29.5 reduce-scatter.5
  136.6 31.1 reduce-scatter.5
  210.5 31.2 reduce-scatter.5
  284.4 31.2 reduce-scatter.5
  358.3 31.2 reduce-scatter.5
